TPU v7x, 32 devices: a whole 2x2x4 slice. The times are simulated.
32 devices in a mesh: grp: 2 (over y), fs: 4 (over z), tp: 4 (over x, core).
Axes of the slice: x: 2, y: 2, z: 4, core: 2. Of those that a mesh axis runs over, the one named last changes fastest.
Arguments:
- tokens: bfloat16 [4096, 2048], P(('grp', 'fs'), 'tp'), parts along dimension 0, may hold values from -6 to 6
- first_gain: bfloat16 [2048], replicated, may hold values from 0.099609375 to 1.8984375
- u_proj: bfloat16 [2048, 1024], P('fs', 'tp'), may hold values from -0.125 to 0.125
- v_proj: bfloat16 [2048, 1024], P('fs', 'tp'), may hold values from -0.125 to 0.125
- group_gain: bfloat16 [8, 128], P('tp'), may hold values from 0.099609375 to 1.8984375
- spatial: bfloat16 [8, 128, 128], P('tp'), may hold values from -0.5 to 0.5
- spatial_bias: bfloat16 [8, 128], P('tp'), may hold values from 0.099609375 to 1.8984375
- mix_proj: bfloat16 [1024, 2048], P('fs', 'tp'), may hold values from -0.1875 to 0.1875
- second_gain: bfloat16 [2048], replicated, may hold values from 0.099609375 to 1.8984375
- up_proj: bfloat16 [2048, 8192], P('fs', 'tp'), may hold values from -0.125 to 0.125
- down_proj: bfloat16 [8192, 2048], P('tp', 'fs'), may hold values from -0.0625 to 0.0625
Outputs:
- layer_out: bfloat16 [4096, 2048], P(('grp', 'fs'), 'tp'), parts along dimension 0
There are 2 independent parts, one for each index of `grp`. A program takes and returns all parts, laid end to end along the dimension named above; an argument that names none is the same for every part. Nothing has to cross between parts.
All inputs are finite; a program needn't handle non-finite values.
Results may differ from a plain program's by a relative error of at most 0.017.
Values may be sent and summed in bfloat16 or wider, within the bound.
A program may use at most 64 MiB of HBM per device.

v0:
```python
import functools

import jax
import jax.numpy as jnp
from jax import lax
from jax.experimental import pallas as pl
from jax.experimental.pallas import tpu as pltpu
from jax.sharding import PartitionSpec as P

EPS = 1e-06


def rms_scale(values, gain_vec):
    mean_sq = jnp.mean(values * values, axis=-1, keepdims=True)
    return values * lax.rsqrt(mean_sq + EPS) * gain_vec.astype(jnp.float32)


def per_device(
    tokens,
    first_gain,
    u_proj,
    v_proj,
    group_gain,
    spatial,
    spatial_bias,
    mix_proj,
    second_gain,
    up_proj,
    down_proj,
):
    whole_rows = lax.all_gather(tokens, "tp", axis=1, tiled=True)
    row_count = whole_rows.shape[0]
    normed_rows = rms_scale(whole_rows.astype(jnp.float32), first_gain).astype(jnp.bfloat16)
    local_width = u_proj.shape[1]
    column_part = normed_rows
    u_pre = jnp.dot(
        column_part,
        lax.all_gather(u_proj, "fs", axis=0, tiled=True),
        preferred_element_type=jnp.float32,
    )
    v_pre = jnp.dot(
        column_part,
        lax.all_gather(v_proj, "fs", axis=0, tiled=True),
        preferred_element_type=jnp.float32,
    )
    u_act = jax.nn.gelu(u_pre).astype(jnp.bfloat16)
    local_groups = group_gain.shape[0]
    group_width = group_gain.shape[1]
    v_groups = jax.nn.gelu(v_pre).reshape(row_count, local_groups, group_width)
    v_normed = rms_scale(v_groups, group_gain).astype(jnp.bfloat16)
    block_len = spatial.shape[1]
    block_view = v_normed.reshape(row_count // block_len, block_len, local_groups, group_width)
    causal_mask = jnp.tril(jnp.ones((block_len, block_len), jnp.bool_))
    masked_weights = jnp.where(causal_mask[None], spatial, jnp.zeros_like(spatial))
    mixed_vals = jnp.einsum(
        "gts,nsgd->ntgd", masked_weights, block_view, preferred_element_type=jnp.float32
    )
    mixed_vals = mixed_vals + spatial_bias.astype(jnp.float32).T[None, :, :, None]
    gated_vals = (u_act.astype(jnp.float32) * mixed_vals.reshape(row_count, local_width)).astype(
        jnp.bfloat16
    )
    gated_whole = lax.all_gather(gated_vals, "tp", axis=1, tiled=True)
    column_part = gated_whole
    mix_vals = jnp.dot(
        column_part,
        lax.all_gather(mix_proj, "fs", axis=0, tiled=True),
        preferred_element_type=jnp.float32,
    )
    mid_stream = (tokens.astype(jnp.float32) + mix_vals).astype(jnp.bfloat16)
    mid_whole = lax.all_gather(mid_stream, "tp", axis=1, tiled=True)
    normed_two = rms_scale(mid_whole.astype(jnp.float32), second_gain).astype(jnp.bfloat16)
    column_part = normed_two
    pre_act = jnp.dot(
        column_part,
        lax.all_gather(up_proj, "fs", axis=0, tiled=True),
        preferred_element_type=jnp.float32,
    )
    hidden_act = jnp.square(jax.nn.relu(pre_act)).astype(jnp.bfloat16)
    down_terms = jnp.dot(
        hidden_act,
        lax.all_gather(down_proj, "fs", axis=1, tiled=True),
        preferred_element_type=jnp.float32,
    )
    down_sum = lax.psum_scatter(
        down_terms.astype(jnp.bfloat16), "tp", scatter_dimension=1, tiled=True
    ).astype(jnp.float32)
    return (mid_stream.astype(jnp.float32) + down_sum).astype(jnp.bfloat16)


def remote(src, dst, send, recv, where):
    return pltpu.make_async_remote_copy(
        src_ref=src,
        dst_ref=dst,
        send_sem=send,
        recv_sem=recv,
        device_id=where,
        device_id_type=pl.DeviceIdType.MESH,
    )


def fused_kernel(
    row_step,
    tok, gain1, u_w, v_w, ggain, spat, bias, mix_w, gain2, up_w, down_w,
    out,
    xg, uvg, mg, upg, dng, norm, gat, mid, hid, c_out, c_in, z_out, z_in, x_out, x_in,
    z_send, z_recv, y_send, y_recv, l_sem, a_send, a_recv, c_send, c_recv, r_send, r_recv,
    s_send, s_recv,
):
    y, z, t = lax.axis_index("grp"), lax.axis_index("fs"), lax.axis_index("tp")
    q, c, x = lax.rem(z, 2), lax.rem(t, 2), t // 2
    z_pair = z + 1 - 2 * q
    t_core, t_chip = t + 1 - 2 * c, lax.rem(t + 2, 4)
    to_y, to_z = (1 - y, z, t), (y, z_pair, t)
    to_c, to_x = (y, z, t_core), (y, z, t_chip)
    across, facing, pair = others = (lax.rem(z + 2, 4), 3 - z, z_pair)
    rows, width = tok.shape
    step = row_step
    f32, bf16 = jnp.float32, jnp.bfloat16

    barrier = pltpu.get_barrier_semaphore()
    for where in (to_y, to_c, to_x) + tuple((y, o, t) for o in others):
        pl.semaphore_signal(
            barrier, inc=1, device_id=where, device_id_type=pl.DeviceIdType.MESH
        )
    pl.semaphore_wait(barrier, 6)

    gw, da = ggain.shape[1], u_w.shape[1]
    ur, mr, pr, dr = u_w.shape[0], mix_w.shape[0], up_w.shape[0], down_w.shape[0] // 2

    def half(size, which):
        return pl.ds(pl.multiple_of(which * size, size), size)

    parts = (1, 1, 1, 2, 2)

    def take(w, par, which, k=0):
        shard = (u_w, v_w, mix_w, up_w, down_w)[w]
        if w == 4:
            if which is None:
                return shard.at[half(dr, par), :]
            return shard.at[half(dr // 4, 4 * par + 2 * which + k), :]
        tall = shard.shape[0]
        cols = slice(None) if w < 3 else half(shard.shape[1] // 2, par)
        if which is None:
            return shard.at[:, cols]
        return shard.at[half(tall // 2 // parts[w], parts[w] * which + k), cols]

    def put(w, source, which, k=0):
        n = parts[w]
        if w == 4:
            if which is None:
                return dng.at[source]
            return dng.at[source, half(dr // 2 // n, n * which + k), :]
        whole, tall = ((uvg, ur), (uvg, ur), (mg, mr), (upg, pr))[w]
        cols = pl.ds(w * da, da) if w < 2 else slice(None)
        if which is None:
            return whole.at[half(tall, source), cols]
        return whole.at[half(tall // 2 // n, n * (2 * source + which) + k), cols]

    def z_piece(w, dest, k):
        return remote(
            take(w, lax.rem(dest, 2), y, k), put(w, z, y, k), z_send.at[w, dest, k],
            z_recv.at[w, z, k], (y, dest, t),
        )

    def z_send_all(w, dest):
        for k in range(parts[w]):
            z_piece(w, dest, k).start()

    def y_piece(w, source, k):
        ref = put(w, source, y, k)
        return remote(ref, ref, y_send.at[w, source, k], y_recv.at[w, source, k], to_y)

    def y_arrived(w, source):
        for k in range(parts[w]):
            ref = put(w, source, 1 - y, k)
            remote(
                ref, ref, y_send.at[w, source, k], y_recv.at[w, source, k], to_y
            ).wait_recv()

    def forward(w, source):
        for k in range(parts[w]):
            ref = put(w, source, y, k)
            remote(
                ref, ref, z_send.at[w, source, k], z_recv.at[w, source, k], (y, source, t)
            ).wait_recv()
            y_piece(w, source, k).start()

    def pass_on(w):
        ref = put(w, across, y)
        remote(
            ref, ref, z_send.at[w, facing, 0], z_recv.at[w, across, 0], (y, pair, t)
        ).start()

    def own_copy(w):
        return pltpu.make_async_copy(take(w, q, None), put(w, z, None), l_sem.at[w])

    def gather_copy(a, h, n):
        p, s, where = (
            (q, t, to_z), (q, t, to_x), (q, t, to_c), (1 - q, t, to_x), (1 - q, t, to_c),
            (q, t_chip, to_c), (1 - q, t_chip, to_c),
        )[n]
        ref = piece(a, h, p, s)
        return remote(ref, ref, a_send.at[a, h, n], a_recv.at[a, h, n], where)

    def gather_arrived(a, h, n):
        p, s, where = (
            (1 - q, t, to_z), (q, t_chip, to_x), (q, t_core, to_c), (1 - q, t_chip, to_x),
            (1 - q, t_core, to_c), (q, 3 - t, to_c), (1 - q, 3 - t, to_c),
        )[n]
        ref = piece(a, h, p, s)
        return remote(ref, ref, a_send.at[a, h, n], a_recv.at[a, h, n], where)

    def piece(a, h, p, s):
        if a == 0:
            return xg.at[s, pl.ds(h * step, step), :]
        return gat.at[s, h] if a == 1 else mid.at[p, s, h]

    def gather_start(a, h):
        for n in (1, 2, 0)[: 3 if a == 2 else 2]:
            gather_copy(a, h, n).start()

    def gather_pair(a, h):
        gather_arrived(a, h, 0).wait_recv()
        gather_copy(a, h, 3).start()
        gather_copy(a, h, 4).start()

    def gather_rest(a, h):
        gather_arrived(a, h, 1).wait_recv()
        gather_copy(a, h, 5).start()
        if a == 2:
            gather_arrived(a, h, 3).wait_recv()
            gather_copy(a, h, 6).start()
        for n in (2, 4, 5, 6) if a == 2 else (2, 5):
            gather_arrived(a, h, n).wait_recv()

    chunks = rows // step
    inner = (z + 1) // 2 == 1

    own_tok = pltpu.make_async_copy(tok, xg.at[t], l_sem.at[5])
    own_tok.start()
    for o in (across, pair):
        for w in range(2):
            z_send_all(w, o)
    own_tok.wait()
    for h in range(chunks):
        gather_start(0, h)
    for w in range(5):
        own_copy(w).start()

    @pl.when(inner)
    def _():
        z_send_all(3, facing)

    for w in range(2):
        forward(w, across)
        pass_on(w)
    z_send_all(2, across)
    z_send_all(2, pair)
    for w in range(2):
        forward(w, pair)

    def scaled(pieces, gain):
        total = pieces[0].shape[0]
        sums = jnp.zeros((total, 1), f32)
        for piece in pieces:
            sums += jnp.sum(piece * piece, axis=-1, keepdims=True)
        count = sum(piece.shape[1] for piece in pieces)
        scale = lax.rsqrt(sums / count + EPS)
        at = 0
        res = []
        for piece in pieces:
            wide = piece.shape[1]
            res.append((piece * scale * gain[:, at : at + wide]).astype(bf16))
            at += wide
        return jnp.concatenate(res, axis=1)

    small = 64
    per_part = step // small
    gain_one = gain1[...].astype(f32).reshape(1, -1)
    gain_two = gain2[...].astype(f32).reshape(1, -1)

    def norm_one(h):
        def loop(i, carry):
            here = pl.ds(pl.multiple_of(h * step + i * small, small), small)
            norm[here, :] = scaled([xg[s, here, :].astype(f32) for s in range(4)], gain_one)
            return carry

        lax.fori_loop(0, per_part, loop, 0)

    blk = spat.shape[1]
    lower = lax.broadcasted_iota(jnp.int32, (blk, blk), 0) >= lax.broadcasted_iota(
        jnp.int32, (blk, blk), 1
    )
    eye = lax.broadcasted_iota(jnp.int32, (blk, blk), 0) == lax.broadcasted_iota(
        jnp.int32, (blk, blk), 1
    )
    mixers, shifts, gains = [], [], []
    for g in range(da // gw):
        mixers.append(jnp.where(lower, spat[g].astype(f32), 0.0).astype(bf16))
        column = jnp.where(eye, bias[g : g + 1, :].astype(f32), 0.0)
        shifts.append(jnp.sum(column, axis=1, keepdims=True))
        gains.append(ggain[g : g + 1, :].astype(f32))

    def mix_rows(h):
        both = jnp.dot(norm[pl.ds(h * step, step), :], uvg[...], preferred_element_type=f32)
        both = jax.nn.gelu(both)
        u_act = both[:, :da].astype(bf16).astype(f32)
        for g in range(da // gw):
            cols = slice(g * gw, (g + 1) * gw)
            v_act = both[:, da + g * gw : da + (g + 1) * gw]
            v_n = (
                v_act
                * lax.rsqrt(jnp.mean(v_act * v_act, axis=-1, keepdims=True) + EPS)
                * gains[g]
            ).astype(bf16)
            for b in range(step // blk):
                part = slice(b * blk, (b + 1) * blk)
                mixed = jnp.dot(mixers[g], v_n[part], preferred_element_type=f32) + shifts[g]
                gat[t, h, part, cols] = (u_act[part, cols] * mixed).astype(bf16)

    def middle_rows(h):
        left = jnp.concatenate([gat[k, h] for k in range(4)], axis=1)
        value = jnp.dot(left, mg[...], preferred_element_type=f32)
        value += tok[pl.ds(h * step, step), :].astype(f32)
        mid[q, t, h] = value.astype(bf16)

    def norm_two(h):
        def loop(i, carry):
            p, r = i // per_part, pl.multiple_of(lax.rem(i, per_part) * small, small)
            pieces = [mid[p, k, h, pl.ds(r, small), :].astype(f32) for k in range(4)]
            at = pl.multiple_of(h * 2 * step + i * small, small)
            norm[pl.ds(at, small), :] = scaled(pieces, gain_two)
            return carry

        lax.fori_loop(0, 2 * per_part, loop, 0)

    def up_rows(h):
        def loop(i, carry):
            here = pl.ds(pl.multiple_of((2 * h + i) * step, step), step)
            pre = jnp.dot(norm[here, :], upg[...], preferred_element_type=f32)
            hid[here, :] = jnp.square(jax.nn.relu(pre)).astype(bf16)
            return carry

        lax.fori_loop(0, 2, loop, 0)

    for h in range(chunks):
        gather_rest(0, h)
        norm_one(h)
    forward(2, across)
    pass_on(2)
    z_send_all(3, across)
    for w in range(2):
        forward(w, facing)
    for w in range(2):
        own_copy(w).wait()
        for o in others:
            y_arrived(w, o)
    for h in range(chunks):
        mix_rows(h)
        gather_start(1, h)
    forward(2, pair)
    forward(2, facing)

    @pl.when(inner)
    def _():
        z_send_all(4, facing)
        forward(3, facing)

    own_copy(2).wait()
    for h in range(chunks):
        gather_rest(1, h)
        if h == 0:
            for o in others:
                y_arrived(2, o)
        middle_rows(h)
        gather_start(2, h)
    forward(3, across)
    for h in range(chunks):
        gather_pair(2, h)

    @pl.when(jnp.logical_not(inner))
    def _():
        z_send_all(3, facing)

    z_send_all(3, pair)
    z_send_all(4, across)
    z_send_all(4, pair)

    @pl.when(jnp.logical_not(inner))
    def _():
        z_send_all(4, facing)

    for h in range(chunks):
        gather_rest(2, h)
        norm_two(h)

    @pl.when(inner)
    def _():
        forward(4, facing)

    @pl.when(jnp.logical_not(inner))
    def _():
        forward(3, facing)

    forward(3, pair)
    forward(4, across)
    own_copy(3).wait()
    for o in others:
        y_arrived(3, o)
    for h in range(chunks):
        up_rows(h)

    near, far = z // 2, 1 - z // 2
    order = (2 * near + 1 - c, 2 * near + c, 2 * far + 1 - c, 2 * far + c)

    def ready(quarter):
        @pl.when(quarter == z)
        def _():
            own_copy(4).wait()

        @pl.when(quarter != z)
        def _():
            y_arrived(4, quarter)

    def down_part(quarter, h, p):
        start = pl.multiple_of((2 * h + p) * step, step)
        return jnp.dot(
            hid[pl.ds(start, step), :], dng[quarter], preferred_element_type=f32
        )

    def core_copy(n, h, p):
        return remote(
            c_out.at[n, h, p], c_in.at[n, h, p], c_send.at[n, h, p], c_recv.at[n, h, p], to_c
        )

    def pair_copy(n, h):
        return remote(z_out.at[n, h], z_in.at[n, h], r_send.at[n, h], r_recv.at[n, h], to_z)

    def chip_copy(h):
        return remote(x_out.at[h], x_in.at[h], s_send.at[h], s_recv.at[h], to_x)

    def give(n):
        quarter = order[2 * n]
        ready(quarter)
        for i in range(2 * chunks):
            h, p = i % chunks, (1 - q if i < chunks else q)
            c_out[n, h, p] = down_part(quarter, h, p).astype(bf16)
            core_copy(n, h, p).start()

    def keep(n):
        quarter = order[2 * n + 1]
        ready(quarter)
        for i in range(2 * chunks):
            h, p = i % chunks, (1 - q if i < chunks else q)
            core_copy(n, h, p).wait_recv()
            value = down_part(quarter, h, p) + c_in[n, h, p].astype(f32)
            if i < chunks:
                z_out[n, h] = value.astype(bf16)
                pair_copy(n, h).start()
            else:
                c_in[n, h, p] = value.astype(bf16)

    forward(4, pair)
    give(0)

    @pl.when(jnp.logical_not(inner))
    def _():
        forward(4, facing)

    keep(0)
    give(1)
    keep(1)

    far_slot = jnp.where(near == x, 1, 0)
    own_slot = 1 - far_slot

    def send_far(n):
        for h in range(chunks):
            pair_copy(n, h).wait_recv()
            value = c_in[n, h, q].astype(f32) + z_in[n, h].astype(f32)
            x_out[h] = value.astype(bf16)
            chip_copy(h).start()

    @pl.when(far_slot == 0)
    def _():
        send_far(0)
        for h in range(chunks):
            pair_copy(1, h).wait_recv()

    @pl.when(far_slot == 1)
    def _():
        for h in range(chunks):
            pair_copy(0, h).wait_recv()
        send_far(1)

    for h in range(chunks):
        chip_copy(h).wait_recv()
        value = c_in[own_slot, h, q].astype(f32) + z_in[own_slot, h].astype(f32)
        value += x_in[h].astype(f32)
        out[pl.ds(h * step, step), :] = (value + mid[q, t, h].astype(f32)).astype(bf16)

    for w in range(5):
        for o in others:
            for k in range(parts[w]):
                z_piece(w, o, k).wait_send()
                y_piece(w, o, k).wait_send()
    for h in range(chunks):
        for a in range(3):
            for n in range(7) if a == 2 else (1, 2, 5):
                gather_copy(a, h, n).wait_send()
        for n in range(2):
            for p in range(2):
                core_copy(n, h, p).wait_send()
            pair_copy(n, h).wait_send()
        chip_copy(h).wait_send()


def fused(tokens, first_gain, u_proj, v_proj, group_gain, spatial, spatial_bias, mix_proj,
          second_gain, up_proj, down_proj):
    rows, width = tokens.shape
    both, wide, da = 2 * rows, second_gain.shape[0], u_proj.shape[1]
    vmem, bf16, dma = pltpu.VMEM, jnp.bfloat16, pltpu.SemaphoreType.DMA
    spec = pl.BlockSpec(memory_space=pltpu.VMEM)
    ff = up_proj.shape[1] // 2
    step = 256
    chunks = rows // step
    return pl.pallas_call(
        functools.partial(fused_kernel, step),
        out_shape=jax.ShapeDtypeStruct(tokens.shape, tokens.dtype),
        in_specs=[spec] * 11,
        out_specs=spec,
        scratch_shapes=[
            vmem((4, rows, width), bf16),
            vmem((wide, 2 * da), bf16),
            vmem((4 * mix_proj.shape[0], width), bf16),
            vmem((wide, ff), bf16),
            vmem((4, ff, down_proj.shape[1]), bf16),
            vmem((both, wide), bf16),
            vmem((4, chunks, step, da), bf16),
            vmem((2, 4, chunks, step, width), bf16),
            vmem((both, ff), bf16),
            vmem((2, chunks, 2, step, width), bf16),
            vmem((2, chunks, 2, step, width), bf16),
            vmem((2, chunks, step, width), bf16),
            vmem((2, chunks, step, width), bf16),
            vmem((chunks, step, width), bf16),
            vmem((chunks, step, width), bf16),
            dma((5, 4, 2)), dma((5, 4, 2)), dma((5, 4, 2)), dma((5, 4, 2)), dma((6,)),
            dma((3, chunks, 7)), dma((3, chunks, 7)),
            dma((2, chunks, 2)), dma((2, chunks, 2)), dma((2, chunks)), dma((2, chunks)),
            dma((chunks,)), dma((chunks,)),
        ],
        compiler_params=pltpu.CompilerParams(
            collective_id=0, has_side_effects=True, vmem_limit_bytes=64 * 1024 * 1000
        ),
    )(
        tokens, first_gain, u_proj, v_proj, group_gain, spatial, spatial_bias, mix_proj,
        second_gain, up_proj, down_proj,
    )


def layer_part(axes, *args):
    tokens, group_gain, spatial = args[0], args[4], args[5]
    fits = (
        axes["grp"] == 2
        and axes["fs"] == 4
        and axes["tp"] == 4
        and group_gain.shape[0] == 2
        and group_gain.shape[1] % 128 == 0
        and tokens.shape[0] % 256 == 0
        and tokens.shape[1] % 256 == 0
        and tokens.shape[1] == args[10].shape[1]
        and 256 % spatial.shape[1] == 0
    )
    return fused(*args) if fits else per_device(*args)


def solution(mesh):
    return jax.shard_map(
        functools.partial(layer_part, dict(mesh.shape)),
        mesh=mesh,
        in_specs=(
            P(("grp", "fs"), "tp"),
            P(),
            P("fs", "tp"),
            P("fs", "tp"),
            P("tp", None),
            P("tp", None, None),
            P("tp", None),
            P("fs", "tp"),
            P(),
            P("fs", "tp"),
            P("tp", "fs"),
        ),
        out_specs=P(("grp", "fs"), "tp"),
        check_vma=False,
    )
```

profile of v0, /device:TPU:16, one launch (start us, length us, event | category | flops | bytes accessed | tf_op | source)
XLA Modules:
  0.0 170.2 jit_solution(15668925516913592942)
XLA Ops:
  0.0 168.3 %shard_map.109 = bf16[512,512]{1,0:T(8,128)(2,1)} custom-call(bf16[512,512]{1,0:T(8,128)(2,1)} %tok.1, bf16[2048]{0:T(1024)(128)(2,1)} %gain1.1, bf16[512,256]{1,0:T(8,128)(2,1)} %u_w.1, bf16[512,256]{1,0:T(8,128)(2,1)} %v_w.1, bf16[2,128]{1,0:T(2,128)(2,1)} %ggain.1, bf16[2,128,128]{2,1,0:T(8,128)(2,1)} %spat.1, bf16[2,128]{1,0:T(2,128)(2,1)} %bias.1, ...), custom_call_target="tpu_custom_call" | custom-call | tf_op jit(solution)/shard_map/pallas_call | solution.py:527
  168.3 1.9 %copy.13 = bf16[512,512]{1,0:T(8,128)(2,1)} copy(bf16[512,512]{1,0:T(8,128)(2,1)} %shard_map.109) | data formatting | bytes 1048576
where the time goes:
time: 170 us
  Pallas kernels  168 us (99%)
  local copies, waits for them, and re-layouts  1.87 us (1%)
    pallas_call x1, Pallas kernels, fused(): pl.pallas_call(functools.partial(fused_kernel, step), out_shape=jax.Shape...  168 us

commit v1 on v0

--- a/solution.py
+++ b/solution.py
@@ -102,9 +102,10 @@
     row_step,
     tok, gain1, u_w, v_w, ggain, spat, bias, mix_w, gain2, up_w, down_w,
     out,
-    xg, uvg, mg, upg, dng, norm, gat, mid, hid, c_out, c_in, z_out, z_in, x_out, x_in,
-    z_send, z_recv, y_send, y_recv, l_sem, a_send, a_recv, c_send, c_recv, r_send, r_recv,
-    s_send, s_recv,
+    xg, uvg, mg, upg, dng, norm, gat, mid, hid, c_out, c_in, z_out, z_in, z_part, x_in, x_out, x_part,
+    acc,
+    h_send, z_send, z_recv, y_send, y_recv, l_sem, a_send, a_recv, c_send, c_recv, r_send,
+    r_recv, s_send, s_recv, p_send, p_recv, o_send, o_recv,
 ):
     y, z, t = lax.axis_index("grp"), lax.axis_index("fs"), lax.axis_index("tp")
     q, c, x = lax.rem(z, 2), lax.rem(t, 2), t // 2
@@ -114,7 +115,7 @@
     to_c, to_x = (y, z, t_core), (y, z, t_chip)
     across, facing, pair = others = (lax.rem(z + 2, 4), 3 - z, z_pair)
     rows, width = tok.shape
-    step = row_step
+    step, z_count = row_step, dng.shape[0]
     f32, bf16 = jnp.float32, jnp.bfloat16
 
     barrier = pltpu.get_barrier_semaphore()
@@ -125,74 +126,110 @@
     pl.semaphore_wait(barrier, 6)
 
     gw, da = ggain.shape[1], u_w.shape[1]
-    ur, mr, pr, dr = u_w.shape[0], mix_w.shape[0], up_w.shape[0], down_w.shape[0] // 2
+    ur, mr, pr = u_w.shape[0], mix_w.shape[0], up_w.shape[0]
+    ff, inner_ff = up_w.shape[1], hid.shape[1]
+    share = (ff - inner_ff, inner_ff)
 
     def half(size, which):
         return pl.ds(pl.multiple_of(which * size, size), size)
 
-    parts = (1, 1, 1, 2, 2)
-
-    def take(w, par, which, k=0):
+    cuts = dng.shape[1]
+    cut = width // cuts
+    parts = (1, 1, 1, 2, cuts)
+
+    def slab(size, which, start=0):
+        if which is None:
+            return pl.ds(start, size)
+        return pl.ds(pl.multiple_of(start + which * (size // 2), 16), size // 2)
+
+    def take(w, role, which, k=0):
         shard = (u_w, v_w, mix_w, up_w, down_w)[w]
+        size, start = share[role], role * share[0]
         if w == 4:
-            if which is None:
-                return shard.at[half(dr, par), :]
-            return shard.at[half(dr // 4, 4 * par + 2 * which + k), :]
+            return shard.at[slab(size, which, start), pl.ds(k * cut, cut)]
         tall = shard.shape[0]
-        cols = slice(None) if w < 3 else half(shard.shape[1] // 2, par)
+        cols = slice(None) if w < 3 else pl.ds(start, size)
         if which is None:
             return shard.at[:, cols]
         return shard.at[half(tall // 2 // parts[w], parts[w] * which + k), cols]
 
-    def put(w, source, which, k=0):
-        n = parts[w]
+    def put(w, role, source, which, k=0):
+        n, size = parts[w], share[role]
         if w == 4:
-            if which is None:
-                return dng.at[source]
-            return dng.at[source, half(dr // 2 // n, n * which + k), :]
+            return dng.at[source, k, slab(size, which), :]
         whole, tall = ((uvg, ur), (uvg, ur), (mg, mr), (upg, pr))[w]
-        cols = pl.ds(w * da, da) if w < 2 else slice(None)
+        cols = pl.ds(w * da, da) if w < 2 else slice(None) if w < 3 else pl.ds(0, size)
         if which is None:
             return whole.at[half(tall, source), cols]
         return whole.at[half(tall // 2 // n, n * (2 * source + which) + k), cols]
 
-    def z_piece(w, dest, k):
+    def z_piece(w, role, dest, k):
         return remote(
-            take(w, lax.rem(dest, 2), y, k), put(w, z, y, k), z_send.at[w, dest, k],
+            take(w, role, y, k), put(w, role, z, y, k), z_send.at[w, dest, k],
             z_recv.at[w, z, k], (y, dest, t),
         )
 
-    def z_send_all(w, dest):
-        for k in range(parts[w]):
-            z_piece(w, dest, k).start()
-
-    def y_piece(w, source, k):
-        ref = put(w, source, y, k)
+    def z_start(w, role, dest, ks=None):
+        for k in range(parts[w]) if ks is None else ks:
+            z_piece(w, role, dest, k).start()
+
+    def y_piece(w, role, source, k):
+        ref = put(w, role, source, y, k)
         return remote(ref, ref, y_send.at[w, source, k], y_recv.at[w, source, k], to_y)
 
-    def y_arrived(w, source):
-        for k in range(parts[w]):
-            ref = put(w, source, 1 - y, k)
-            remote(
-                ref, ref, y_send.at[w, source, k], y_recv.at[w, source, k], to_y
-            ).wait_recv()
-
-    def forward(w, source):
-        for k in range(parts[w]):
-            ref = put(w, source, y, k)
-            remote(
-                ref, ref, z_send.at[w, source, k], z_recv.at[w, source, k], (y, source, t)
-            ).wait_recv()
-            y_piece(w, source, k).start()
-
-    def pass_on(w):
-        ref = put(w, across, y)
+    def y_arrived(w, role, source, k):
+        ref = put(w, role, source, 1 - y, k)
         remote(
-            ref, ref, z_send.at[w, facing, 0], z_recv.at[w, across, 0], (y, pair, t)
-        ).start()
-
-    def own_copy(w):
-        return pltpu.make_async_copy(take(w, q, None), put(w, z, None), l_sem.at[w])
+            ref, ref, y_send.at[w, source, k], y_recv.at[w, source, k], to_y
+        ).wait_recv()
+
+    def y_all(w, role):
+        for o in others:
+            for k in range(parts[w]):
+                y_arrived(w, role, o, k)
+
+    def relay(w, role, source, k):
+        ref = put(w, role, source, y, k)
+        remote(
+            ref, ref, z_send.at[w, source, k], z_recv.at[w, source, k], (y, source, t)
+        ).wait_recv()
+        y_piece(w, role, source, k).start()
+
+    def relays(w, role, source, ks=None):
+        for k in range(parts[w]) if ks is None else ks:
+            relay(w, role, source, k)
+
+    def hop(w, source, way, own=False):
+        ref = put(w, 0, source, y)
+        return remote(
+            take(w, 0, y) if own else ref, ref, h_send.at[w, source, way],
+            z_recv.at[w, source, 0], (y, z + 1 - 2 * way, t),
+        )
+
+    last = z_count - 1
+    goes_on = (z < last, z > 0)
+
+    def chain(w, distance):
+        for way in range(2):
+            source = z - distance if way == 0 else z + distance
+
+            @pl.when(source >= 0 if way == 0 else source <= last)
+            def _():
+                hop(w, source, way).wait_recv()
+
+                @pl.when(goes_on[way])
+                def _():
+                    hop(w, source, way).start()
+
+                y_piece(w, 0, source, 0).start()
+
+    def own_copies(w, role):
+        return [
+            pltpu.make_async_copy(
+                take(w, role, None, k), put(w, role, z, None, k), l_sem.at[w + k]
+            )
+            for k in range(cuts if w == 4 else 1)
+        ]
 
     def gather_copy(a, h, n):
         p, s, where = (
@@ -234,31 +271,18 @@
             gather_arrived(a, h, n).wait_recv()
 
     chunks = rows // step
-    inner = (z + 1) // 2 == 1
-
-    own_tok = pltpu.make_async_copy(tok, xg.at[t], l_sem.at[5])
+    inner = jnp.logical_and(z > 0, z < last)
+
+    own_tok = pltpu.make_async_copy(tok, xg.at[t], l_sem.at[4 + cuts])
     own_tok.start()
-    for o in (across, pair):
-        for w in range(2):
-            z_send_all(w, o)
+    for w in range(3):
+        for way in range(2):
+            @pl.when(goes_on[way])
+            def _():
+                hop(w, z, way, True).start()
     own_tok.wait()
     for h in range(chunks):
         gather_start(0, h)
-    for w in range(5):
-        own_copy(w).start()
-
-    @pl.when(inner)
-    def _():
-        z_send_all(3, facing)
-
-    for w in range(2):
-        forward(w, across)
-        pass_on(w)
-    z_send_all(2, across)
-    z_send_all(2, pair)
-    for w in range(2):
-        forward(w, pair)
-
     def scaled(pieces, gain):
         total = pieces[0].shape[0]
         sums = jnp.zeros((total, 1), f32)
@@ -334,185 +358,288 @@
 
         lax.fori_loop(0, 2 * per_part, loop, 0)
 
-    def up_rows(h):
+    def up_rows(h, role):
+        size = share[role]
+
         def loop(i, carry):
             here = pl.ds(pl.multiple_of((2 * h + i) * step, step), step)
-            pre = jnp.dot(norm[here, :], upg[...], preferred_element_type=f32)
-            hid[here, :] = jnp.square(jax.nn.relu(pre)).astype(bf16)
+            pre = jnp.dot(norm[here, :], upg[:, :size], preferred_element_type=f32)
+            hid[here, :size] = jnp.square(jax.nn.relu(pre)).astype(bf16)
             return carry
 
         lax.fori_loop(0, 2, loop, 0)
 
-    for h in range(chunks):
-        gather_rest(0, h)
-        norm_one(h)
-    forward(2, across)
-    pass_on(2)
-    z_send_all(3, across)
-    for w in range(2):
-        forward(w, facing)
-    for w in range(2):
-        own_copy(w).wait()
-        for o in others:
-            y_arrived(w, o)
-    for h in range(chunks):
-        mix_rows(h)
-        gather_start(1, h)
-    forward(2, pair)
-    forward(2, facing)
+    def part(quarter, k, b, role):
+        start, size = pl.multiple_of(b * step, step), share[role]
+        return jnp.dot(
+            hid[pl.ds(start, step), :size], dng[quarter, k, :size],
+            preferred_element_type=f32,
+        )
+
+    def core_copy(n, k):
+        return remote(
+            c_out.at[n, k], c_in.at[n, k], c_send.at[n, k], c_recv.at[n, k], to_c
+        )
+
+    wide_n, slim_n = c, 1 - c
+    own_wide = x == c
+
+    def wide_x(k):
+        return remote(c_in.at[wide_n, k], x_in.at[k], s_send.at[k], s_recv.at[k], to_x)
+
+    def wide_z(k):
+        return remote(z_out.at[k], z_in.at[k], r_send.at[k], r_recv.at[k], to_z)
+
+    def slim_z(k):
+        return remote(
+            c_in.at[slim_n, k, 1 - q], z_part.at[k], p_send.at[k], p_recv.at[k], to_z
+        )
+
+    def slim_x(k):
+        return remote(x_out.at[k], x_part.at[k], o_send.at[k], o_recv.at[k], to_x)
+
+    def down(quarter, k, role):
+        n = quarter // 2
+        mine = lax.rem(quarter, 2) == c
+
+        @pl.when(jnp.logical_not(mine))
+        def _():
+            def loop(b, carry):
+                c_out[n, k, lax.rem(b, 2), b // 2] = part(quarter, k, b, role).astype(bf16)
+                return carry
+
+            lax.fori_loop(0, 2 * chunks, loop, 0)
+            core_copy(n, k).start()
+
+        @pl.when(mine)
+        def _():
+            def loop(b, carry):
+                acc[b] = part(quarter, k, b, role)
+                return carry
+
+            lax.fori_loop(0, 2 * chunks, loop, 0)
+            core_copy(n, k).wait_recv()
+
+            def add(b, carry):
+                p, h = lax.rem(b, 2), b // 2
+                value = acc[b] + c_in[n, k, p, h].astype(f32)
+                c_in[n, k, p, h] = value.astype(bf16)
+                return carry
+
+            lax.fori_loop(0, 2 * chunks, add, 0)
+
+            @pl.when((n == wide_n) & jnp.logical_not(own_wide))
+            def _():
+                wide_x(k).start()
+
+            @pl.when(n == slim_n)
+            def _():
+                slim_z(k).start()
+
+    def meet(role):
+        @pl.when(own_wide)
+        def _():
+            for k in every:
+                wide_x(k).wait_recv()
+                for h in range(chunks):
+                    value = c_in[wide_n, k, 1 - q, h].astype(f32)
+                    value += x_in[k, 1 - q, h].astype(f32)
+                    z_out[k, h] = value.astype(bf16)
+                wide_z(k).start()
+
+    every = range(cuts)
+    early, late = every[: cuts // 2], every[cuts // 2 :]
+
+    def mixer():
+        for w in range(2):
+            for copy in own_copies(w, 0):
+                copy.wait()
+            y_all(w, 0)
+        for h in range(chunks):
+            mix_rows(h)
+            gather_start(1, h)
+
+    def middle():
+        for copy in own_copies(2, 0):
+            copy.wait()
+        y_all(2, 0)
+        for h in range(chunks):
+            gather_rest(1, h)
+            middle_rows(h)
+            gather_start(2, h)
+
+    def widen(role):
+        for copy in own_copies(3, role):
+            copy.wait()
+        y_all(3, role)
+        for h in range(chunks):
+            up_rows(h, role)
+        for copy in own_copies(4, role):
+            copy.wait()
+
+    def downs(role, source, ks=None):
+        for k in every if ks is None else ks:
+            y_arrived(4, role, source, k)
+            down(source, k, role)
+
+    def start(role):
+        for w in range(5):
+            for copy in own_copies(w, role):
+                copy.start()
+
+    @pl.when(jnp.logical_not(inner))
+    def _():
+        start(0)
+        z_start(3, 1, pair)
+        z_start(3, 1, across)
+        z_start(4, 1, across, early)
+        for w in range(3):
+            chain(w, 1)
+        for h in range(chunks):
+            gather_rest(0, h)
+            norm_one(h)
+        for d in range(2, z_count):
+            for w in range(3):
+                chain(w, d)
+        mixer()
+        middle()
+        z_start(4, 1, across, late[:1])
+        z_start(3, 0, facing)
+        z_start(4, 1, pair)
+        z_start(4, 1, across, late[1:])
+        z_start(4, 0, facing)
+        relays(3, 0, pair)
+        gather_pair(2, 0)
+        gather_pair(2, 1)
+        gather_rest(2, 0)
+        norm_two(0)
+        relay(3, 0, facing, 0)
+        gather_rest(2, 1)
+        norm_two(1)
+        relay(3, 0, facing, 1)
+        relays(3, 0, across)
+        widen(0)
+        for k in every:
+            down(z, k, 0)
+        relays(4, 0, pair, early[:1])
+        relays(4, 0, facing)
+        relays(4, 0, across, early)
+        downs(0, facing)
+        relays(4, 0, across, late)
+        downs(0, across)
+        relays(4, 0, pair, every[1:])
+        downs(0, pair)
+        meet(0)
 
     @pl.when(inner)
     def _():
-        z_send_all(4, facing)
-        forward(3, facing)
-
-    own_copy(2).wait()
-    for h in range(chunks):
-        gather_rest(1, h)
-        if h == 0:
-            for o in others:
-                y_arrived(2, o)
-        middle_rows(h)
-        gather_start(2, h)
-    forward(3, across)
-    for h in range(chunks):
-        gather_pair(2, h)
+        start(1)
+        for w in range(3):
+            chain(w, 1)
+        z_start(3, 1, facing)
+        z_start(4, 1, facing, early[:1])
+        z_start(3, 0, across)
+        z_start(4, 0, across)
+        z_start(4, 1, facing, every[1:])
+        for h in range(chunks):
+            gather_rest(0, h)
+            norm_one(h)
+        for w in range(3):
+            chain(w, 2)
+        z_start(3, 0, pair)
+        for w in range(3):
+            chain(w, 3)
+        relays(3, 1, pair)
+        mixer()
+        relays(3, 1, across)
+        middle()
+        z_start(4, 0, pair)
+        relay(3, 1, facing, 0)
+        gather_pair(2, 0)
+        relay(3, 1, facing, 1)
+        gather_pair(2, 1)
+        relays(4, 1, across, early)
+        gather_rest(2, 0)
+        norm_two(0)
+        gather_rest(2, 1)
+        norm_two(1)
+        widen(1)
+        relays(4, 1, across, late)
+        for k in every:
+            down(z, k, 1)
+        relays(4, 1, pair)
+        downs(1, across)
+        downs(1, pair)
+        relays(4, 1, facing)
+        meet(1)
+        downs(1, facing)
+
+    def result(value, k, h):
+        cols = slice(k * cut, (k + 1) * cut)
+        value += mid[q, t, h, :, cols].astype(f32)
+        out[pl.ds(h * step, step), cols] = value.astype(bf16)
+
+    @pl.when(own_wide)
+    def _():
+        for k in every:
+            slim_z(k).wait_recv()
+            for h in range(chunks):
+                value = c_in[slim_n, k, q, h].astype(f32) + z_part[k, h].astype(f32)
+                x_out[k, h] = value.astype(bf16)
+            slim_x(k).start()
+        for k in every:
+            wide_z(k).wait_recv()
+            for h in range(chunks):
+                value = c_in[wide_n, k, q, h].astype(f32) + x_in[k, q, h].astype(f32)
+                result(value + z_in[k, h].astype(f32), k, h)
+        for k in every:
+            wide_z(k).wait_send()
+            slim_x(k).wait_send()
+
+    @pl.when(jnp.logical_not(own_wide))
+    def _():
+        for k in every:
+            slim_z(k).wait_recv()
+            slim_x(k).wait_recv()
+            for h in range(chunks):
+                value = c_in[slim_n, k, q, h].astype(f32) + z_part[k, h].astype(f32)
+                result(value + x_part[k, h].astype(f32), k, h)
+        for k in every:
+            wide_x(k).wait_send()
+
+    def drain(role):
+        for w in range(5):
+            for o, other in ((across, 1 - role), (facing, role), (pair, 1 - role)):
+                for k in range(parts[w]):
+                    if w > 2:
+                        z_piece(w, other, o, k).wait_send()
+                    y_piece(w, role, o, k).wait_send()
 
     @pl.when(jnp.logical_not(inner))
     def _():
-        z_send_all(3, facing)
-
-    z_send_all(3, pair)
-    z_send_all(4, across)
-    z_send_all(4, pair)
-
-    @pl.when(jnp.logical_not(inner))
-    def _():
-        z_send_all(4, facing)
-
-    for h in range(chunks):
-        gather_rest(2, h)
-        norm_two(h)
+        drain(0)
 
     @pl.when(inner)
     def _():
-        forward(4, facing)
-
-    @pl.when(jnp.logical_not(inner))
-    def _():
-        forward(3, facing)
-
-    forward(3, pair)
-    forward(4, across)
-    own_copy(3).wait()
-    for o in others:
-        y_arrived(3, o)
-    for h in range(chunks):
-        up_rows(h)
-
-    near, far = z // 2, 1 - z // 2
-    order = (2 * near + 1 - c, 2 * near + c, 2 * far + 1 - c, 2 * far + c)
-
-    def ready(quarter):
-        @pl.when(quarter == z)
-        def _():
-            own_copy(4).wait()
-
-        @pl.when(quarter != z)
-        def _():
-            y_arrived(4, quarter)
-
-    def down_part(quarter, h, p):
-        start = pl.multiple_of((2 * h + p) * step, step)
-        return jnp.dot(
-            hid[pl.ds(start, step), :], dng[quarter], preferred_element_type=f32
-        )
-
-    def core_copy(n, h, p):
-        return remote(
-            c_out.at[n, h, p], c_in.at[n, h, p], c_send.at[n, h, p], c_recv.at[n, h, p], to_c
-        )
-
-    def pair_copy(n, h):
-        return remote(z_out.at[n, h], z_in.at[n, h], r_send.at[n, h], r_recv.at[n, h], to_z)
-
-    def chip_copy(h):
-        return remote(x_out.at[h], x_in.at[h], s_send.at[h], s_recv.at[h], to_x)
-
-    def give(n):
-        quarter = order[2 * n]
-        ready(quarter)
-        for i in range(2 * chunks):
-            h, p = i % chunks, (1 - q if i < chunks else q)
-            c_out[n, h, p] = down_part(quarter, h, p).astype(bf16)
-            core_copy(n, h, p).start()
-
-    def keep(n):
-        quarter = order[2 * n + 1]
-        ready(quarter)
-        for i in range(2 * chunks):
-            h, p = i % chunks, (1 - q if i < chunks else q)
-            core_copy(n, h, p).wait_recv()
-            value = down_part(quarter, h, p) + c_in[n, h, p].astype(f32)
-            if i < chunks:
-                z_out[n, h] = value.astype(bf16)
-                pair_copy(n, h).start()
-            else:
-                c_in[n, h, p] = value.astype(bf16)
-
-    forward(4, pair)
-    give(0)
-
-    @pl.when(jnp.logical_not(inner))
-    def _():
-        forward(4, facing)
-
-    keep(0)
-    give(1)
-    keep(1)
-
-    far_slot = jnp.where(near == x, 1, 0)
-    own_slot = 1 - far_slot
-
-    def send_far(n):
-        for h in range(chunks):
-            pair_copy(n, h).wait_recv()
-            value = c_in[n, h, q].astype(f32) + z_in[n, h].astype(f32)
-            x_out[h] = value.astype(bf16)
-            chip_copy(h).start()
-
-    @pl.when(far_slot == 0)
-    def _():
-        send_far(0)
-        for h in range(chunks):
-            pair_copy(1, h).wait_recv()
-
-    @pl.when(far_slot == 1)
-    def _():
-        for h in range(chunks):
-            pair_copy(0, h).wait_recv()
-        send_far(1)
-
-    for h in range(chunks):
-        chip_copy(h).wait_recv()
-        value = c_in[own_slot, h, q].astype(f32) + z_in[own_slot, h].astype(f32)
-        value += x_in[h].astype(f32)
-        out[pl.ds(h * step, step), :] = (value + mid[q, t, h].astype(f32)).astype(bf16)
-
-    for w in range(5):
-        for o in others:
-            for k in range(parts[w]):
-                z_piece(w, o, k).wait_send()
-                y_piece(w, o, k).wait_send()
+        drain(1)
+
+    for w in range(3):
+        for source in range(z_count):
+            for way in range(2):
+                came = source <= z if way == 0 else source >= z
+
+                @pl.when(came & goes_on[way])
+                def _():
+                    hop(w, source, way).wait_send()
+
     for h in range(chunks):
         for a in range(3):
             for n in range(7) if a == 2 else (1, 2, 5):
                 gather_copy(a, h, n).wait_send()
+    for k in every:
         for n in range(2):
-            for p in range(2):
-                core_copy(n, h, p).wait_send()
-            pair_copy(n, h).wait_send()
-        chip_copy(h).wait_send()
+            core_copy(n, k).wait_send()
+        slim_z(k).wait_send()
 
 
 def fused(tokens, first_gain, u_proj, v_proj, group_gain, spatial, spatial_bias, mix_proj,
@@ -521,9 +648,11 @@
     both, wide, da = 2 * rows, second_gain.shape[0], u_proj.shape[1]
     vmem, bf16, dma = pltpu.VMEM, jnp.bfloat16, pltpu.SemaphoreType.DMA
     spec = pl.BlockSpec(memory_space=pltpu.VMEM)
-    ff = up_proj.shape[1] // 2
+    ff = up_proj.shape[1] // 16 * 9
     step = 256
     chunks = rows // step
+    cuts = 4
+    cut = width // cuts
     return pl.pallas_call(
         functools.partial(fused_kernel, step),
         out_shape=jax.ShapeDtypeStruct(tokens.shape, tokens.dtype),
@@ -534,21 +663,26 @@
             vmem((wide, 2 * da), bf16),
             vmem((4 * mix_proj.shape[0], width), bf16),
             vmem((wide, ff), bf16),
-            vmem((4, ff, down_proj.shape[1]), bf16),
+            vmem((4, cuts, ff, cut), bf16),
             vmem((both, wide), bf16),
             vmem((4, chunks, step, da), bf16),
             vmem((2, 4, chunks, step, width), bf16),
             vmem((both, ff), bf16),
-            vmem((2, chunks, 2, step, width), bf16),
-            vmem((2, chunks, 2, step, width), bf16),
-            vmem((2, chunks, step, width), bf16),
-            vmem((2, chunks, step, width), bf16),
-            vmem((chunks, step, width), bf16),
-            vmem((chunks, step, width), bf16),
-            dma((5, 4, 2)), dma((5, 4, 2)), dma((5, 4, 2)), dma((5, 4, 2)), dma((6,)),
+            vmem((2, cuts, 2, chunks, step, cut), bf16),
+            vmem((2, cuts, 2, chunks, step, cut), bf16),
+            vmem((cuts, chunks, step, cut), bf16),
+            vmem((cuts, chunks, step, cut), bf16),
+            vmem((cuts, chunks, step, cut), bf16),
+            vmem((cuts, 2, chunks, step, cut), bf16),
+            vmem((cuts, chunks, step, cut), bf16),
+            vmem((cuts, chunks, step, cut), bf16),
+            vmem((2 * chunks, step, cut), jnp.float32),
+            dma((3, 4, 2)),
+            dma((5, 4, 4)), dma((5, 4, 4)), dma((5, 4, 4)), dma((5, 4, 4)), dma((5 + cuts,)),
             dma((3, chunks, 7)), dma((3, chunks, 7)),
-            dma((2, chunks, 2)), dma((2, chunks, 2)), dma((2, chunks)), dma((2, chunks)),
-            dma((chunks,)), dma((chunks,)),
+            dma((2, cuts)), dma((2, cuts)), dma((cuts,)), dma((cuts,)),
+            dma((cuts,)), dma((cuts,)), dma((cuts,)), dma((cuts,)), dma((cuts,)),
+            dma((cuts,)),
         ],
         compiler_params=pltpu.CompilerParams(
             collective_id=0, has_side_effects=True, vmem_limit_bytes=64 * 1024 * 1000
@@ -571,6 +705,7 @@
         and tokens.shape[1] % 256 == 0
         and tokens.shape[1] == args[10].shape[1]
         and 256 % spatial.shape[1] == 0
+        and args[9].shape[1] % 2048 == 0
     )
     return fused(*args) if fits else per_device(*args)
 

time: 170 us -> 153 us (0.900)
  the two profiles are of different devices: /device:TPU:16 before, /device:TPU:0 now
where the time goes in v1:
time: 153 us
  Pallas kernels  151 us (99%)
  local copies, waits for them, and re-layouts  1.87 us (1%)
    pallas_call x1, Pallas kernels, fused(): pl.pallas_call(functools.partial(fused_kernel, step), out_shape=jax.Shape...  151 us

profile of v1, /device:TPU:0, one launch (start us, length us, event | category | flops | bytes accessed | tf_op | source)
XLA Modules:
  0.0 153.0 jit_solution(10203031609174526639)
XLA Ops:
  0.0 151.1 %shard_map.109 = bf16[512,512]{1,0:T(8,128)(2,1)} custom-call(bf16[512,512]{1,0:T(8,128)(2,1)} %tok.1, bf16[2048]{0:T(1024)(128)(2,1)} %gain1.1, bf16[512,256]{1,0:T(8,128)(2,1)} %u_w.1, bf16[512,256]{1,0:T(8,128)(2,1)} %v_w.1, bf16[2,128]{1,0:T(2,128)(2,1)} %ggain.1, bf16[2,128,128]{2,1,0:T(8,128)(2,1)} %spat.1, bf16[2,128]{1,0:T(2,128)(2,1)} %bias.1, ...), custom_call_target="tpu_custom_call" | custom-call | tf_op jit(solution)/shard_map/pallas_call | solution.py:656
  151.1 1.9 %copy.13 = bf16[512,512]{1,0:T(8,128)(2,1)} copy(bf16[512,512]{1,0:T(8,128)(2,1)} %shard_map.109) | data formatting | bytes 1048576

commit v2 on v1

--- a/solution.py
+++ b/solution.py
@@ -99,7 +99,7 @@
 
 
 def fused_kernel(
-    row_step,
+    row_step, piece_cuts,
     tok, gain1, u_w, v_w, ggain, spat, bias, mix_w, gain2, up_w, down_w,
     out,
     xg, uvg, mg, upg, dng, norm, gat, mid, hid, c_out, c_in, z_out, z_in, z_part, x_in, x_out, x_part,
@@ -133,9 +133,12 @@
     def half(size, which):
         return pl.ds(pl.multiple_of(which * size, size), size)
 
-    cuts = dng.shape[1]
-    cut = width // cuts
+    cuts, cut = piece_cuts, width // piece_cuts
+    cols, col = c_out.shape[1], c_out.shape[3]
     parts = (1, 1, 1, 2, cuts)
+
+    def lane(w, k):
+        return sum(parts[:w]) + k
 
     def slab(size, which, start=0):
         if which is None:
@@ -146,7 +149,8 @@
         shard = (u_w, v_w, mix_w, up_w, down_w)[w]
         size, start = share[role], role * share[0]
         if w == 4:
-            return shard.at[slab(size, which, start), pl.ds(k * cut, cut)]
+            wide = pl.ds(0, width) if which is None else pl.ds(k * cut, cut)
+            return shard.at[slab(size, which, start), wide]
         tall = shard.shape[0]
         cols = slice(None) if w < 3 else pl.ds(start, size)
         if which is None:
@@ -156,7 +160,8 @@
     def put(w, role, source, which, k=0):
         n, size = parts[w], share[role]
         if w == 4:
-            return dng.at[source, k, slab(size, which), :]
+            wide = pl.ds(0, width) if which is None else pl.ds(k * cut, cut)
+            return dng.at[source, slab(size, which), wide]
         whole, tall = ((uvg, ur), (uvg, ur), (mg, mr), (upg, pr))[w]
         cols = pl.ds(w * da, da) if w < 2 else slice(None) if w < 3 else pl.ds(0, size)
         if which is None:
@@ -165,8 +170,8 @@
 
     def z_piece(w, role, dest, k):
         return remote(
-            take(w, role, y, k), put(w, role, z, y, k), z_send.at[w, dest, k],
-            z_recv.at[w, z, k], (y, dest, t),
+            take(w, role, y, k), put(w, role, z, y, k), z_send.at[lane(w, k), dest],
+            z_recv.at[lane(w, k), z], (y, dest, t),
         )
 
     def z_start(w, role, dest, ks=None):
@@ -175,12 +180,12 @@
 
     def y_piece(w, role, source, k):
         ref = put(w, role, source, y, k)
-        return remote(ref, ref, y_send.at[w, source, k], y_recv.at[w, source, k], to_y)
+        return remote(ref, ref, y_send.at[lane(w, k), source], y_recv.at[lane(w, k), source], to_y)
 
     def y_arrived(w, role, source, k):
         ref = put(w, role, source, 1 - y, k)
         remote(
-            ref, ref, y_send.at[w, source, k], y_recv.at[w, source, k], to_y
+            ref, ref, y_send.at[lane(w, k), source], y_recv.at[lane(w, k), source], to_y
         ).wait_recv()
 
     def y_all(w, role):
@@ -191,7 +196,7 @@
     def relay(w, role, source, k):
         ref = put(w, role, source, y, k)
         remote(
-            ref, ref, z_send.at[w, source, k], z_recv.at[w, source, k], (y, source, t)
+            ref, ref, z_send.at[lane(w, k), source], z_recv.at[lane(w, k), source], (y, source, t)
         ).wait_recv()
         y_piece(w, role, source, k).start()
 
@@ -203,7 +208,7 @@
         ref = put(w, 0, source, y)
         return remote(
             take(w, 0, y) if own else ref, ref, h_send.at[w, source, way],
-            z_recv.at[w, source, 0], (y, z + 1 - 2 * way, t),
+            z_recv.at[lane(w, 0), source], (y, z + 1 - 2 * way, t),
         )
 
     last = z_count - 1
@@ -223,12 +228,23 @@
 
                 y_piece(w, 0, source, 0).start()
 
+    def chain_pair(w):
+        way = 1 - q
+        hop(w, pair, way).wait_recv()
+        hop(w, pair, way).start()
+        y_piece(w, 0, pair, 0).start()
+
+    def chain_facing(w):
+        way = q
+        hop(w, facing, way).wait_recv()
+        hop(w, facing, way).start()
+        y_piece(w, 0, facing, 0).start()
+
     def own_copies(w, role):
         return [
             pltpu.make_async_copy(
-                take(w, role, None, k), put(w, role, z, None, k), l_sem.at[w + k]
+                take(w, role, None), put(w, role, z, None), l_sem.at[w]
             )
-            for k in range(cuts if w == 4 else 1)
         ]
 
     def gather_copy(a, h, n):
@@ -250,7 +266,7 @@
     def piece(a, h, p, s):
         if a == 0:
             return xg.at[s, pl.ds(h * step, step), :]
-        return gat.at[s, h] if a == 1 else mid.at[p, s, h]
+        return gat.at[s, h] if a == 1 else mid.at[p, s, pl.ds(h * step, step)]
 
     def gather_start(a, h):
         for n in (1, 2, 0)[: 3 if a == 2 else 2]:
@@ -273,13 +289,16 @@
     chunks = rows // step
     inner = jnp.logical_and(z > 0, z < last)
 
-    own_tok = pltpu.make_async_copy(tok, xg.at[t], l_sem.at[4 + cuts])
+    own_tok = pltpu.make_async_copy(tok, xg.at[t], l_sem.at[5])
     own_tok.start()
-    for w in range(3):
+    def hop_own(w):
         for way in range(2):
             @pl.when(goes_on[way])
             def _():
                 hop(w, z, way, True).start()
+
+    hop_own(0)
+    hop_own(1)
     own_tok.wait()
     for h in range(chunks):
         gather_start(0, h)
@@ -346,13 +365,14 @@
         left = jnp.concatenate([gat[k, h] for k in range(4)], axis=1)
         value = jnp.dot(left, mg[...], preferred_element_type=f32)
         value += tok[pl.ds(h * step, step), :].astype(f32)
-        mid[q, t, h] = value.astype(bf16)
+        mid[q, t, pl.ds(h * step, step)] = value.astype(bf16)
 
     def norm_two(h):
         def loop(i, carry):
             p, r = i // per_part, pl.multiple_of(lax.rem(i, per_part) * small, small)
-            pieces = [mid[p, k, h, pl.ds(r, small), :].astype(f32) for k in range(4)]
-            at = pl.multiple_of(h * 2 * step + i * small, small)
+            here = pl.ds(pl.multiple_of(h * step + r, small), small)
+            pieces = [mid[p, k, here, :].astype(f32) for k in range(4)]
+            at = pl.multiple_of((p * chunks + h) * step + r, small)
             norm[pl.ds(at, small), :] = scaled(pieces, gain_two)
             return carry
 
@@ -362,19 +382,21 @@
         size = share[role]
 
         def loop(i, carry):
-            here = pl.ds(pl.multiple_of((2 * h + i) * step, step), step)
+            here = pl.ds(pl.multiple_of((i * chunks + h) * step, step), step)
             pre = jnp.dot(norm[here, :], upg[:, :size], preferred_element_type=f32)
             hid[here, :size] = jnp.square(jax.nn.relu(pre)).astype(bf16)
             return carry
 
         lax.fori_loop(0, 2, loop, 0)
 
-    def part(quarter, k, b, role):
-        start, size = pl.multiple_of(b * step, step), share[role]
+    def part(quarter, k, p, role):
+        size, side = share[role], slice(k * col, (k + 1) * col)
         return jnp.dot(
-            hid[pl.ds(start, step), :size], dng[quarter, k, :size],
-            preferred_element_type=f32,
+            hid[half_rows(p), :size], dng[quarter, :size, side], preferred_element_type=f32
         )
+
+    def half_rows(p):
+        return pl.ds(pl.multiple_of(p * rows, rows), rows)
 
     def core_copy(n, k):
         return remote(
@@ -392,7 +414,7 @@
 
     def slim_z(k):
         return remote(
-            c_in.at[slim_n, k, 1 - q], z_part.at[k], p_send.at[k], p_recv.at[k], to_z
+            c_in.at[slim_n, k, half_rows(1 - q)], z_part.at[k], p_send.at[k], p_recv.at[k], to_z
         )
 
     def slim_x(k):
@@ -404,29 +426,29 @@
 
         @pl.when(jnp.logical_not(mine))
         def _():
-            def loop(b, carry):
-                c_out[n, k, lax.rem(b, 2), b // 2] = part(quarter, k, b, role).astype(bf16)
+            def loop(p, carry):
+                c_out[n, k, half_rows(p), :] = part(quarter, k, p, role).astype(bf16)
                 return carry
 
-            lax.fori_loop(0, 2 * chunks, loop, 0)
+            lax.fori_loop(0, 2, loop, 0)
             core_copy(n, k).start()
 
         @pl.when(mine)
         def _():
-            def loop(b, carry):
-                acc[b] = part(quarter, k, b, role)
+            def loop(p, carry):
+                acc[half_rows(p), :] = part(quarter, k, p, role)
                 return carry
 
-            lax.fori_loop(0, 2 * chunks, loop, 0)
+            lax.fori_loop(0, 2, loop, 0)
             core_copy(n, k).wait_recv()
 
             def add(b, carry):
-                p, h = lax.rem(b, 2), b // 2
-                value = acc[b] + c_in[n, k, p, h].astype(f32)
-                c_in[n, k, p, h] = value.astype(bf16)
+                here = pl.ds(pl.multiple_of(b * small, small), small)
+                value = acc[here, :] + c_in[n, k, here, :].astype(f32)
+                c_in[n, k, here, :] = value.astype(bf16)
                 return carry
 
-            lax.fori_loop(0, 2 * chunks, add, 0)
+            lax.fori_loop(0, 2 * rows // small, add, 0)
 
             @pl.when((n == wide_n) & jnp.logical_not(own_wide))
             def _():
@@ -436,19 +458,34 @@
             def _():
                 slim_z(k).start()
 
+    sides = range(cols)
+
+    def in_rows(run):
+        def loop(b, carry):
+            run(
+                pl.ds(pl.multiple_of(b * small, small), small),
+                pl.ds(pl.multiple_of((1 - q) * rows + b * small, small), small),
+                pl.ds(pl.multiple_of(q * rows + b * small, small), small),
+            )
+            return carry
+
+        lax.fori_loop(0, rows // small, loop, 0)
+
     def meet(role):
         @pl.when(own_wide)
         def _():
-            for k in every:
+            for k in sides:
                 wide_x(k).wait_recv()
-                for h in range(chunks):
-                    value = c_in[wide_n, k, 1 - q, h].astype(f32)
-                    value += x_in[k, 1 - q, h].astype(f32)
-                    z_out[k, h] = value.astype(bf16)
+
+                def run(here, theirs, ours):
+                    value = c_in[wide_n, k, theirs, :].astype(f32)
+                    value += x_in[k, theirs, :].astype(f32)
+                    z_out[k, here, :] = value.astype(bf16)
+
+                in_rows(run)
                 wide_z(k).start()
 
     every = range(cuts)
-    early, late = every[: cuts // 2], every[cuts // 2 :]
 
     def mixer():
         for w in range(2):
@@ -468,18 +505,18 @@
             middle_rows(h)
             gather_start(2, h)
 
-    def widen(role):
+    def up_ready(role):
         for copy in own_copies(3, role):
             copy.wait()
         y_all(3, role)
-        for h in range(chunks):
-            up_rows(h, role)
         for copy in own_copies(4, role):
             copy.wait()
 
     def downs(role, source, ks=None):
-        for k in every if ks is None else ks:
-            y_arrived(4, role, source, k)
+        per = cuts // cols
+        for k in sides if ks is None else ks:
+            for i in range(per):
+                y_arrived(4, role, source, k * per + i)
             down(source, k, role)
 
     def start(role):
@@ -489,25 +526,29 @@
 
     @pl.when(jnp.logical_not(inner))
     def _():
+        hop_own(2)
         start(0)
         z_start(3, 1, pair)
         z_start(3, 1, across)
-        z_start(4, 1, across, early)
-        for w in range(3):
+        for w in range(2):
             chain(w, 1)
         for h in range(chunks):
             gather_rest(0, h)
             norm_one(h)
-        for d in range(2, z_count):
-            for w in range(3):
-                chain(w, d)
+        for w in range(2):
+            chain(w, 2)
+        chain(2, 1)
+        for w in range(2):
+            chain(w, 3)
+        chain(2, 2)
+        chain(2, 3)
         mixer()
         middle()
-        z_start(4, 1, across, late[:1])
+        z_start(4, 1, across, every[:1])
         z_start(3, 0, facing)
         z_start(4, 1, pair)
-        z_start(4, 1, across, late[1:])
         z_start(4, 0, facing)
+        z_start(4, 1, across, every[1:])
         relays(3, 0, pair)
         gather_pair(2, 0)
         gather_pair(2, 1)
@@ -518,93 +559,127 @@
         norm_two(1)
         relay(3, 0, facing, 1)
         relays(3, 0, across)
-        widen(0)
-        for k in every:
-            down(z, k, 0)
-        relays(4, 0, pair, early[:1])
-        relays(4, 0, facing)
-        relays(4, 0, across, early)
+        relay(4, 0, across, 0)
+        relay(4, 0, across, 1)
+        up_ready(0)
+        relay(4, 0, facing, 0)
+        relay(4, 0, facing, 1)
+        up_rows(0, 0)
+        relay(4, 0, facing, 2)
+        relay(4, 0, facing, 3)
+        up_rows(1, 0)
+        relay(4, 0, pair, 0)
+        down(z, 0, 0)
+        relay(4, 0, pair, 1)
+        down(z, 1, 0)
+        downs(0, across, sides[:1])
+        relay(4, 0, pair, 2)
         downs(0, facing)
-        relays(4, 0, across, late)
-        downs(0, across)
-        relays(4, 0, pair, every[1:])
+        relay(4, 0, across, 2)
+        relay(4, 0, across, 3)
+        relay(4, 0, pair, 3)
         downs(0, pair)
+        downs(0, across, sides[1:])
         meet(0)
 
     @pl.when(inner)
     def _():
         start(1)
-        for w in range(3):
-            chain(w, 1)
+        for w in range(2):
+            chain_pair(w)
+            chain_facing(w)
+        hop_own(2)
+        chain_pair(2)
         z_start(3, 1, facing)
-        z_start(4, 1, facing, early[:1])
+        z_start(4, 1, facing, every[:1])
         z_start(3, 0, across)
         z_start(4, 0, across)
         z_start(4, 1, facing, every[1:])
+        for w in range(2):
+            chain(w, 2)
+        chain_facing(2)
         for h in range(chunks):
             gather_rest(0, h)
             norm_one(h)
-        for w in range(3):
-            chain(w, 2)
+        chain(2, 2)
         z_start(3, 0, pair)
-        for w in range(3):
-            chain(w, 3)
         relays(3, 1, pair)
         mixer()
-        relays(3, 1, across)
+        relay(3, 1, across, 0)
         middle()
         z_start(4, 0, pair)
+        relay(3, 1, across, 1)
         relay(3, 1, facing, 0)
+        relay(3, 1, facing, 1)
         gather_pair(2, 0)
-        relay(3, 1, facing, 1)
         gather_pair(2, 1)
-        relays(4, 1, across, early)
+        relay(4, 1, facing, 0)
+        relay(4, 1, across, 0)
         gather_rest(2, 0)
         norm_two(0)
         gather_rest(2, 1)
         norm_two(1)
-        widen(1)
-        relays(4, 1, across, late)
-        for k in every:
-            down(z, k, 1)
-        relays(4, 1, pair)
+        relay(4, 1, pair, 0)
+        up_ready(1)
+        relay(4, 1, pair, 1)
+        up_rows(0, 1)
+        relay(4, 1, pair, 2)
+        up_rows(1, 1)
+        relay(4, 1, pair, 3)
+        down(z, 0, 1)
+        down(z, 1, 1)
+        downs(1, pair)
+        relay(4, 1, across, 1)
+        relay(4, 1, across, 2)
+        relay(4, 1, across, 3)
+        relay(4, 1, facing, 1)
         downs(1, across)
-        downs(1, pair)
-        relays(4, 1, facing)
+        relays(4, 1, facing, every[2:])
         meet(1)
         downs(1, facing)
 
-    def result(value, k, h):
-        cols = slice(k * cut, (k + 1) * cut)
-        value += mid[q, t, h, :, cols].astype(f32)
-        out[pl.ds(h * step, step), cols] = value.astype(bf16)
+    def result(value, k, here):
+        side = slice(k * col, (k + 1) * col)
+        out[here, side] = (value + residual(here, side)).astype(bf16)
+
+    def residual(here, side):
+        return mid[q, t, here, side].astype(f32)
 
     @pl.when(own_wide)
     def _():
-        for k in every:
+        for k in sides:
             slim_z(k).wait_recv()
-            for h in range(chunks):
-                value = c_in[slim_n, k, q, h].astype(f32) + z_part[k, h].astype(f32)
-                x_out[k, h] = value.astype(bf16)
+
+            def run(here, theirs, ours):
+                value = c_in[slim_n, k, ours, :].astype(f32) + z_part[k, here, :].astype(f32)
+                x_out[k, here, :] = value.astype(bf16)
+
+            in_rows(run)
             slim_x(k).start()
-        for k in every:
+        for k in sides:
             wide_z(k).wait_recv()
-            for h in range(chunks):
-                value = c_in[wide_n, k, q, h].astype(f32) + x_in[k, q, h].astype(f32)
-                result(value + z_in[k, h].astype(f32), k, h)
-        for k in every:
+
+            def run(here, theirs, ours):
+                value = c_in[wide_n, k, ours, :].astype(f32) + x_in[k, ours, :].astype(f32)
+                result(value + z_in[k, here, :].astype(f32), k, here)
+
+            in_rows(run)
+        for k in sides:
             wide_z(k).wait_send()
             slim_x(k).wait_send()
 
     @pl.when(jnp.logical_not(own_wide))
     def _():
-        for k in every:
+        for k in sides:
             slim_z(k).wait_recv()
             slim_x(k).wait_recv()
-            for h in range(chunks):
-                value = c_in[slim_n, k, q, h].astype(f32) + z_part[k, h].astype(f32)
-                result(value + x_part[k, h].astype(f32), k, h)
-        for k in every:
+
+            def run(here, theirs, ours):
+                value = c_in[slim_n, k, ours, :].astype(f32) + z_part[k, here, :].astype(f32)
+                result(value + x_part[k, here, :].astype(f32), k, here)
+
+            in_rows(run)
+        for k in sides:
             wide_x(k).wait_send()
 
     def drain(role):
@@ -636,7 +711,7 @@
         for a in range(3):
             for n in range(7) if a == 2 else (1, 2, 5):
                 gather_copy(a, h, n).wait_send()
-    for k in every:
+    for k in sides:
         for n in range(2):
             core_copy(n, k).wait_send()
         slim_z(k).wait_send()
@@ -652,9 +727,10 @@
     step = 256
     chunks = rows // step
     cuts = 4
-    cut = width // cuts
+    cols = 2
+    col = width // cols
     return pl.pallas_call(
-        functools.partial(fused_kernel, step),
+        functools.partial(fused_kernel, step, cuts),
         out_shape=jax.ShapeDtypeStruct(tokens.shape, tokens.dtype),
         in_specs=[spec] * 11,
         out_specs=spec,
@@ -663,26 +739,26 @@
             vmem((wide, 2 * da), bf16),
             vmem((4 * mix_proj.shape[0], width), bf16),
             vmem((wide, ff), bf16),
-            vmem((4, cuts, ff, cut), bf16),
+            vmem((4, ff, width), bf16),
             vmem((both, wide), bf16),
             vmem((4, chunks, step, da), bf16),
-            vmem((2, 4, chunks, step, width), bf16),
+            vmem((2, 4, rows, width), bf16),
             vmem((both, ff), bf16),
-            vmem((2, cuts, 2, chunks, step, cut), bf16),
-            vmem((2, cuts, 2, chunks, step, cut), bf16),
-            vmem((cuts, chunks, step, cut), bf16),
-            vmem((cuts, chunks, step, cut), bf16),
-            vmem((cuts, chunks, step, cut), bf16),
-            vmem((cuts, 2, chunks, step, cut), bf16),
-            vmem((cuts, chunks, step, cut), bf16),
-            vmem((cuts, chunks, step, cut), bf16),
-            vmem((2 * chunks, step, cut), jnp.float32),
+            vmem((2, cols, both, col), bf16),
+            vmem((2, cols, both, col), bf16),
+            vmem((cols, rows, col), bf16),
+            vmem((cols, rows, col), bf16),
+            vmem((cols, rows, col), bf16),
+            vmem((cols, both, col), bf16),
+            vmem((cols, rows, col), bf16),
+            vmem((cols, rows, col), bf16),
+            vmem((both, col), jnp.float32),
             dma((3, 4, 2)),
-            dma((5, 4, 4)), dma((5, 4, 4)), dma((5, 4, 4)), dma((5, 4, 4)), dma((5 + cuts,)),
+            dma((5 + cuts, 4)), dma((5 + cuts, 4)), dma((5 + cuts, 4)), dma((5 + cuts, 4)),
+            dma((6,)),
             dma((3, chunks, 7)), dma((3, chunks, 7)),
-            dma((2, cuts)), dma((2, cuts)), dma((cuts,)), dma((cuts,)),
-            dma((cuts,)), dma((cuts,)), dma((cuts,)), dma((cuts,)), dma((cuts,)),
-            dma((cuts,)),
+            dma((2, cols)), dma((2, cols)), dma((cols,)), dma((cols,)), dma((cols,)),
+            dma((cols,)), dma((cols,)), dma((cols,)), dma((cols,)), dma((cols,)),
         ],
         compiler_params=pltpu.CompilerParams(
             collective_id=0, has_side_effects=True, vmem_limit_bytes=64 * 1024 * 1000

time: 153 us -> 141 us (0.922)
  Pallas kernels: 151 us -> 138 us
    pallas_call x1, Pallas kernels: 151 us -> 138 us  [fused(): pl.pallas_call(functools.partial(fused_kernel, step, cuts), out_shape=jax...]
where the time goes in v2:
time: 141 us; the launch traced here: 140 us
  Pallas kernels  138 us (98%)
  local copies, waits for them, and re-layouts  1.87 us (1%)
    pallas_call x1, Pallas kernels, fused(): pl.pallas_call(functools.partial(fused_kernel, step, cuts), out_shape=jax...  138 us

profile of v2, /device:TPU:0, one launch (start us, length us, event | category | flops | bytes accessed | tf_op | source)
XLA Modules:
  0.0 140.1 jit_solution(2881407001208290052)
XLA Ops:
  0.0 138.2 %shard_map.109 = bf16[512,512]{1,0:T(8,128)(2,1)} custom-call(bf16[512,512]{1,0:T(8,128)(2,1)} %tok.1, bf16[2048]{0:T(1024)(128)(2,1)} %gain1.1, bf16[512,256]{1,0:T(8,128)(2,1)} %u_w.1, bf16[512,256]{1,0:T(8,128)(2,1)} %v_w.1, bf16[2,128]{1,0:T(2,128)(2,1)} %ggain.1, bf16[2,128,128]{2,1,0:T(8,128)(2,1)} %spat.1, bf16[2,128]{1,0:T(2,128)(2,1)} %bias.1, ...), custom_call_target="tpu_custom_call" | custom-call | tf_op jit(solution)/shard_map/pallas_call | solution.py:732
  138.2 1.9 %copy.13 = bf16[512,512]{1,0:T(8,128)(2,1)} copy(bf16[512,512]{1,0:T(8,128)(2,1)} %shard_map.109) | data formatting | bytes 1048576

commit v3 on v2

--- a/solution.py
+++ b/solution.py
@@ -118,6 +118,8 @@
     step, z_count = row_step, dng.shape[0]
     f32, bf16 = jnp.float32, jnp.bfloat16
 
+    own_tok = pltpu.make_async_copy(tok, xg.at[t], l_sem.at[5])
+    own_tok.start()
     barrier = pltpu.get_barrier_semaphore()
     for where in (to_y, to_c, to_x) + tuple((y, o, t) for o in others):
         pl.semaphore_signal(
@@ -170,7 +172,7 @@
 
     def z_piece(w, role, dest, k):
         return remote(
-            take(w, role, y, k), put(w, role, z, y, k), z_send.at[lane(w, k), dest],
+            take(w, role, y, k), put(w, role, z, y, k), z_send.at[lane(w, k) - 3, dest],
             z_recv.at[lane(w, k), z], (y, dest, t),
         )
 
@@ -196,7 +198,7 @@
     def relay(w, role, source, k):
         ref = put(w, role, source, y, k)
         remote(
-            ref, ref, z_send.at[lane(w, k), source], z_recv.at[lane(w, k), source], (y, source, t)
+            ref, ref, z_send.at[lane(w, k) - 3, source], z_recv.at[lane(w, k), source], (y, source, t)
         ).wait_recv()
         y_piece(w, role, source, k).start()
 
@@ -247,13 +249,16 @@
             )
         ]
 
+    def link(a, n):
+        return 6 + n if a == 2 else 3 * a + (1, 2, 5).index(n)
+
     def gather_copy(a, h, n):
         p, s, where = (
             (q, t, to_z), (q, t, to_x), (q, t, to_c), (1 - q, t, to_x), (1 - q, t, to_c),
             (q, t_chip, to_c), (1 - q, t_chip, to_c),
         )[n]
         ref = piece(a, h, p, s)
-        return remote(ref, ref, a_send.at[a, h, n], a_recv.at[a, h, n], where)
+        return remote(ref, ref, a_send.at[link(a, n), h], a_recv.at[link(a, n), h], where)
 
     def gather_arrived(a, h, n):
         p, s, where = (
@@ -261,7 +266,7 @@
             (1 - q, t_core, to_c), (q, 3 - t, to_c), (1 - q, 3 - t, to_c),
         )[n]
         ref = piece(a, h, p, s)
-        return remote(ref, ref, a_send.at[a, h, n], a_recv.at[a, h, n], where)
+        return remote(ref, ref, a_send.at[link(a, n), h], a_recv.at[link(a, n), h], where)
 
     def piece(a, h, p, s):
         if a == 0:
@@ -289,8 +294,6 @@
     chunks = rows // step
     inner = jnp.logical_and(z > 0, z < last)
 
-    own_tok = pltpu.make_async_copy(tok, xg.at[t], l_sem.at[5])
-    own_tok.start()
     def hop_own(w):
         for way in range(2):
             @pl.when(goes_on[way])
@@ -364,7 +367,7 @@
     def middle_rows(h):
         left = jnp.concatenate([gat[k, h] for k in range(4)], axis=1)
         value = jnp.dot(left, mg[...], preferred_element_type=f32)
-        value += tok[pl.ds(h * step, step), :].astype(f32)
+        value += xg[t, pl.ds(h * step, step), :].astype(f32)
         mid[q, t, pl.ds(h * step, step)] = value.astype(bf16)
 
     def norm_two(h):
@@ -459,6 +462,7 @@
                 slim_z(k).start()
 
     sides = range(cols)
+    low, high = sides[: cols // 2], sides[cols // 2 :]
 
     def in_rows(run):
         def loop(b, carry):
@@ -471,10 +475,10 @@
 
         lax.fori_loop(0, rows // small, loop, 0)
 
-    def meet(role):
-        @pl.when(own_wide)
+    def meet(ks, fits=True):
+        @pl.when(own_wide & fits)
         def _():
-            for k in sides:
+            for k in ks:
                 wide_x(k).wait_recv()
 
                 def run(here, theirs, ours):
@@ -518,6 +522,15 @@
             for i in range(per):
                 y_arrived(4, role, source, k * per + i)
             down(source, k, role)
+
+    def last_downs(role, k):
+        per = cuts // cols
+        for source in (pair, across):
+            for i in range(per):
+                y_arrived(4, role, source, k * per + i)
+        pair_first = lax.rem(pair, 2) != c
+        down(jnp.where(pair_first, pair, across), k, role)
+        down(jnp.where(pair_first, across, pair), k, role)
 
     def start(role):
         for w in range(5):
@@ -569,18 +582,22 @@
         relay(4, 0, facing, 3)
         up_rows(1, 0)
         relay(4, 0, pair, 0)
-        down(z, 0, 0)
+        for k in low:
+            down(z, k, 0)
         relay(4, 0, pair, 1)
-        down(z, 1, 0)
-        downs(0, across, sides[:1])
+        for k in high:
+            down(z, k, 0)
+        downs(0, across, low)
         relay(4, 0, pair, 2)
         downs(0, facing)
         relay(4, 0, across, 2)
         relay(4, 0, across, 3)
         relay(4, 0, pair, 3)
-        downs(0, pair)
-        downs(0, across, sides[1:])
-        meet(0)
+        downs(0, pair, low)
+        meet(low)
+        for k in high:
+            last_downs(0, k)
+        meet(high)
 
     @pl.when(inner)
     def _():
@@ -626,17 +643,21 @@
         relay(4, 1, pair, 2)
         up_rows(1, 1)
         relay(4, 1, pair, 3)
-        down(z, 0, 1)
-        down(z, 1, 1)
+        for k in low:
+            down(z, k, 1)
+        for k in high:
+            down(z, k, 1)
         downs(1, pair)
         relay(4, 1, across, 1)
         relay(4, 1, across, 2)
         relay(4, 1, across, 3)
+        downs(1, across, low)
         relay(4, 1, facing, 1)
-        downs(1, across)
+        downs(1, across, high)
         relays(4, 1, facing, every[2:])
-        meet(1)
+        meet(sides, t == pair)
         downs(1, facing)
+        meet(sides, t == across)
 
     def result(value, k, here):
         side = slice(k * col, (k + 1) * col)
@@ -722,17 +743,17 @@
     rows, width = tokens.shape
     both, wide, da = 2 * rows, second_gain.shape[0], u_proj.shape[1]
     vmem, bf16, dma = pltpu.VMEM, jnp.bfloat16, pltpu.SemaphoreType.DMA
-    spec = pl.BlockSpec(memory_space=pltpu.VMEM)
+    spec, far = (pl.BlockSpec(memory_space=m) for m in (pltpu.VMEM, pl.ANY))
     ff = up_proj.shape[1] // 16 * 9
     step = 256
     chunks = rows // step
     cuts = 4
-    cols = 2
+    cols = 4
     col = width // cols
     return pl.pallas_call(
         functools.partial(fused_kernel, step, cuts),
         out_shape=jax.ShapeDtypeStruct(tokens.shape, tokens.dtype),
-        in_specs=[spec] * 11,
+        in_specs=[far, spec, far, far, spec, spec, spec, far, spec, far, far],
         out_specs=spec,
         scratch_shapes=[
             vmem((4, rows, width), bf16),
@@ -754,9 +775,9 @@
             vmem((cols, rows, col), bf16),
             vmem((both, col), jnp.float32),
             dma((3, 4, 2)),
-            dma((5 + cuts, 4)), dma((5 + cuts, 4)), dma((5 + cuts, 4)), dma((5 + cuts, 4)),
+            dma((2 + cuts, 4)), dma((5 + cuts, 4)), dma((5 + cuts, 4)), dma((5 + cuts, 4)),
             dma((6,)),
-            dma((3, chunks, 7)), dma((3, chunks, 7)),
+            dma((13, chunks)), dma((13, chunks)),
             dma((2, cols)), dma((2, cols)), dma((cols,)), dma((cols,)), dma((cols,)),
             dma((cols,)), dma((cols,)), dma((cols,)), dma((cols,)), dma((cols,)),
         ],

time: 141 us -> 135 us (0.957)
  Pallas kernels: 138 us -> 133 us
    pallas_call x1, Pallas kernels: 138 us -> 133 us  [fused(): pl.pallas_call(functools.partial(fused_kernel, step, cuts), out_shape=jax...]
where the time goes in v3:
time: 135 us
  Pallas kernels  133 us (99%)
  local copies, waits for them, and re-layouts  1.87 us (1%)
    pallas_call x1, Pallas kernels, fused(): pl.pallas_call(functools.partial(fused_kernel, step, cuts), out_shape=jax...  133 us

profile of v3, /device:TPU:0, one launch (start us, length us, event | category | flops | bytes accessed | tf_op | source)
XLA Modules:
  0.0 135.2 jit_solution(15883981690731888875)
XLA Ops:
  0.0 133.3 %shard_map.109 = bf16[512,512]{1,0:T(8,128)(2,1)} custom-call(bf16[512,512]{1,0:T(8,128)(2,1)} %tok.1, bf16[2048]{0:T(1024)(128)(2,1)} %gain1.1, bf16[512,256]{1,0:T(8,128)(2,1)} %u_w.1, bf16[512,256]{1,0:T(8,128)(2,1)} %v_w.1, bf16[2,128]{1,0:T(2,128)(2,1)} %ggain.1, bf16[2,128,128]{2,1,0:T(8,128)(2,1)} %spat.1, bf16[2,128]{1,0:T(2,128)(2,1)} %bias.1, ...), custom_call_target="tpu_custom_call" | custom-call | tf_op jit(solution)/shard_map/pallas_call | solution.py:753
  133.3 1.9 %copy.13 = bf16[512,512]{1,0:T(8,128)(2,1)} copy(bf16[512,512]{1,0:T(8,128)(2,1)} %shard_map.109) | data formatting | bytes 1048576

commit v4 on v3

--- a/solution.py
+++ b/solution.py
@@ -100,8 +100,9 @@
 
 def fused_kernel(
     row_step, piece_cuts,
-    tok, gain1, u_w, v_w, ggain, spat, bias, mix_w, gain2, up_w, down_w,
+    tok, far_gain1, u_w, v_w, far_ggain, far_spat, far_bias, mix_w, far_gain2, up_w, down_w,
     out,
+    gain1, ggain, spat, bias, gain2,
     xg, uvg, mg, upg, dng, norm, gat, mid, hid, c_out, c_in, z_out, z_in, z_part, x_in, x_out, x_part,
     acc,
     h_send, z_send, z_recv, y_send, y_recv, l_sem, a_send, a_recv, c_send, c_recv, r_send,
@@ -120,6 +121,15 @@
 
     own_tok = pltpu.make_async_copy(tok, xg.at[t], l_sem.at[5])
     own_tok.start()
+    fetches = [
+        pltpu.make_async_copy(held, near, l_sem.at[6 + i])
+        for i, (held, near) in enumerate((
+            (far_gain1, gain1), (far_ggain, ggain), (far_spat, spat), (far_bias, bias),
+            (far_gain2, gain2),
+        ))
+    ]
+    for fetch in fetches:
+        fetch.start()
     barrier = pltpu.get_barrier_semaphore()
     for where in (to_y, to_c, to_x) + tuple((y, o, t) for o in others):
         pl.semaphore_signal(
@@ -305,6 +315,9 @@
     own_tok.wait()
     for h in range(chunks):
         gather_start(0, h)
+    for fetch in fetches:
+        fetch.wait()
+
     def scaled(pieces, gain):
         total = pieces[0].shape[0]
         sums = jnp.zeros((total, 1), f32)
@@ -745,6 +758,7 @@
     vmem, bf16, dma = pltpu.VMEM, jnp.bfloat16, pltpu.SemaphoreType.DMA
     spec, far = (pl.BlockSpec(memory_space=m) for m in (pltpu.VMEM, pl.ANY))
     ff = up_proj.shape[1] // 16 * 9
+    small = (first_gain, group_gain, spatial, spatial_bias, second_gain)
     step = 256
     chunks = rows // step
     cuts = 4
@@ -753,9 +767,10 @@
     return pl.pallas_call(
         functools.partial(fused_kernel, step, cuts),
         out_shape=jax.ShapeDtypeStruct(tokens.shape, tokens.dtype),
-        in_specs=[far, spec, far, far, spec, spec, spec, far, spec, far, far],
+        in_specs=[far] * 11,
         out_specs=spec,
         scratch_shapes=[
+            *(vmem(v.shape, v.dtype) for v in small),
             vmem((4, rows, width), bf16),
             vmem((wide, 2 * da), bf16),
             vmem((4 * mix_proj.shape[0], width), bf16),
@@ -776,7 +791,7 @@
             vmem((both, col), jnp.float32),
             dma((3, 4, 2)),
             dma((2 + cuts, 4)), dma((5 + cuts, 4)), dma((5 + cuts, 4)), dma((5 + cuts, 4)),
-            dma((6,)),
+            dma((11,)),
             dma((13, chunks)), dma((13, chunks)),
             dma((2, cols)), dma((2, cols)), dma((cols,)), dma((cols,)), dma((cols,)),
             dma((cols,)), dma((cols,)), dma((cols,)), dma((cols,)), dma((cols,)),

time: 135 us -> 135 us (level)
  no operation moved by 1% of the time
where the time goes in v4:
time: 135 us; the launch traced here: 134 us
  Pallas kernels  132 us (98%)
  local copies, waits for them, and re-layouts  1.87 us (1%)
    pallas_call x1, Pallas kernels, fused(): pl.pallas_call(functools.partial(fused_kernel, step, cuts), out_shape=jax...  132 us

profile of v4, /device:TPU:0, one launch (start us, length us, event | category | flops | bytes accessed | tf_op | source)
XLA Modules:
  0.0 134.4 jit_solution(2029202085764908576)
XLA Ops:
  0.0 132.5 %shard_map.109 = bf16[512,512]{1,0:T(8,128)(2,1)} custom-call(bf16[512,512]{1,0:T(8,128)(2,1)} %tok.1, bf16[2048]{0:T(1024)(128)(2,1)} %far_gain1.1, bf16[512,256]{1,0:T(8,128)(2,1)} %u_w.1, bf16[512,256]{1,0:T(8,128)(2,1)} %v_w.1, bf16[2,128]{1,0:T(2,128)(2,1)} %far_ggain.1, bf16[2,128,128]{2,1,0:T(8,128)(2,1)} %far_spat.1, bf16[2,128]{1,0:T(2,128)(2,1)} %far_bias.1, ...), custom_call_target="tpu_custom_call" | custom-call | tf_op jit(solution)/shard_map/pallas_call | solution.py:767
  132.5 1.9 %copy.13 = bf16[512,512]{1,0:T(8,128)(2,1)} copy(bf16[512,512]{1,0:T(8,128)(2,1)} %shard_map.109) | data formatting | bytes 1048576
